TPU v7x, 32 devices: a whole 2x2x4 slice. The times are simulated.
32 devices in a mesh: sp: 8 (over z, x), tp: 4 (over y, core).
Axes of the slice: x: 2, y: 2, z: 4, core: 2. Of those that a mesh axis runs over, the one named last changes fastest.
Arguments:
- residual: bfloat16 [1536, 2048], P('sp', 'tp'), may hold values from -10 to 10
- queries: bfloat16 [1536, 16, 128], P('sp', 'tp'), may hold values from -6.5 to 6.5
- key_rows: bfloat16 [1536, 16, 128], P('sp', 'tp'), may hold values from -6.5 to 6.5
- value_rows: bfloat16 [1536, 16, 128], P('sp', 'tp'), may hold values from -6 to 6
- diff_scale: float32 [16], P('tp'), may hold values from 0.3 to 0.8
- head_gain: float32 [128], replicated, may hold values from 0.1 to 1.9
- out_weight: bfloat16 [2048, 2048], P(None, 'tp'), may hold values from -0.125 to 0.125
- norm_gain: float32 [2048], replicated, may hold values from 0.1 to 1.9
- gate_weight: bfloat16 [8, 2048, 4096], P('sp', None, 'tp'), may hold values from -0.5 to 0.5
- up_weight: bfloat16 [8, 2048, 4096], P('sp', None, 'tp'), may hold values from -0.5 to 0.5
- down_weight: bfloat16 [8, 4096, 2048], P('sp', None, 'tp'), may hold values from -0.01171875 to 0.01171875
- expert_ids: int32 [1536, 2], P('sp'), may hold values from 0 to 7, all different within a row; in each aligned block of 192 rows (0 to 191, 192 to 383, ...) at most 96 rows name the same one
- route_logit: float32 [1536, 2], P('sp'), may hold values from -6 to 6
Outputs:
- updated: bfloat16 [1536, 2048], P('sp', 'tp')
Inputs may be any that keep to these rules, and one draw needn't show every extreme that they name: `expert_ids`: A token's 2 experts differ. The 192 tokens of one index of sp name one expert at most 96 times, a bound that some block reaches on some index.
All inputs are finite; a program needn't handle non-finite values.
Results may differ from a plain program's by a relative error of at most 0.014.
Values may be sent and summed in bfloat16 or wider, within the bound.
A program may use at most 64 MiB of HBM per device.

v0:
```python
import math
import jax
import jax.numpy as jnp
from jax import lax
from jax.sharding import PartitionSpec as P

D = 2048
QK = 64
SPAN = 64
NORM_EPS = 1e-05
CLAMP_LIMIT = 7.0
SWISH_ALPHA = 1.702
HEAD_KEEP = 0.8
NEG_FILL = -1e30


def update_map(running, query_half, key_half, value_block, visible):
    row_peak, row_total, accum = running
    scores = jnp.einsum(
        "qhd,khd->hqk", query_half, key_half, preferred_element_type=jnp.float32
    ) * QK ** (-0.5)
    scores = jnp.where(visible[None], scores, NEG_FILL)
    new_peak = jnp.maximum(row_peak, jnp.max(scores, axis=-1))
    exp_weights = jnp.where(visible[None], jnp.exp(scores - new_peak[..., None]), 0.0)
    rescale = jnp.exp(row_peak - new_peak)
    row_total = row_total * rescale + jnp.sum(exp_weights, axis=-1)
    accum = accum * rescale[..., None] + jnp.einsum(
        "hqk,khv->hqv",
        exp_weights.astype(jnp.bfloat16),
        value_block,
        preferred_element_type=jnp.float32,
    )
    return (new_peak, row_total, accum)


def local(
    residual,
    queries,
    key_rows,
    value_rows,
    diff_scale,
    head_gain,
    out_weight,
    norm_gain,
    gate_weight,
    up_weight,
    down_weight,
    expert_ids,
    route_logit,
):
    tokens_here = queries.shape[0]
    heads_here = queries.shape[1]
    value_width = value_rows.shape[2]
    query_start = lax.axis_index("sp") * tokens_here
    query_span = (query_start + jnp.arange(tokens_here, dtype=jnp.int32)) // SPAN
    first_query = queries[..., :QK]
    second_query = queries[..., QK:]
    empty_map = (
        jnp.full((heads_here, tokens_here), NEG_FILL, jnp.float32),
        jnp.zeros((heads_here, tokens_here), jnp.float32),
        jnp.zeros((heads_here, tokens_here, value_width), jnp.float32),
    )
    folded = (empty_map, empty_map)
    key_piece = lax.all_gather(key_rows, "sp", axis=0, tiled=True)
    value_piece = lax.all_gather(value_rows, "sp", axis=0, tiled=True)
    key_count = key_piece.shape[0]
    key_width = math.gcd(key_count, 1024)
    blocks = key_count // key_width
    key_blocks = key_piece.reshape(blocks, key_width, heads_here, 2 * QK)
    value_blocks = value_piece.reshape(blocks, key_width, heads_here, value_width)

    def advance(running, inputs):
        block_index, key_block, value_block = inputs
        key_start = block_index * key_width

        def compute(current):
            key_span = (key_start + jnp.arange(key_width, dtype=jnp.int32)) // SPAN
            visible = key_span[None, :] <= query_span[:, None]
            first = update_map(current[0], first_query, key_block[..., :QK], value_block, visible)
            second = update_map(current[1], second_query, key_block[..., QK:], value_block, visible)
            return (first, second)

        running = lax.cond(
            key_start < query_start + tokens_here, compute, lambda current: current, running
        )
        return (running, None)

    folded, _ = lax.scan(
        advance, folded, (jnp.arange(blocks, dtype=jnp.int32), key_blocks, value_blocks)
    )
    first_map, second_map = folded
    mixture = (
        first_map[2] / first_map[1][..., None]
        - diff_scale[:, None, None] * second_map[2] / second_map[1][..., None]
    )
    scale_back = lax.rsqrt(jnp.mean(mixture * mixture, axis=-1, keepdims=True) + NORM_EPS)
    attended = (mixture * scale_back * head_gain * HEAD_KEEP).astype(jnp.bfloat16)
    column_width = out_weight.shape[1]
    head_weight = out_weight.reshape(-1, value_width, column_width)
    weight_slice = head_weight
    projected = jnp.einsum(
        "htv,hvd->td",
        lax.all_gather(attended, "tp", axis=0, tiled=True),
        weight_slice,
        preferred_element_type=jnp.float32,
    )
    after_mixer = (residual.astype(jnp.float32) + projected).astype(jnp.bfloat16)
    mixer_float = after_mixer.astype(jnp.float32)
    partial_value = jnp.sum(mixer_float * mixer_float, axis=-1)
    square_total = lax.psum(partial_value, "tp")
    gain_slice = lax.dynamic_slice_in_dim(
        norm_gain, lax.axis_index("tp") * column_width, column_width, 0
    )
    normed = (mixer_float * lax.rsqrt(square_total / D + NORM_EPS)[:, None] * gain_slice).astype(
        jnp.bfloat16
    )
    experts = lax.axis_size("sp")
    top_count = expert_ids.shape[1]
    capacity = 2 * tokens_here * top_count // experts
    chosen = expert_ids.reshape(-1)
    onehot = (chosen[:, None] == jnp.arange(experts, dtype=jnp.int32)[None, :]).astype(jnp.int32)
    rank_in = jnp.sum(jnp.cumsum(onehot, axis=0) * onehot, axis=1) - 1
    slot_index = chosen * capacity + rank_in
    owner_row = (
        jnp.full((experts * capacity,), tokens_here, jnp.int32)
        .at[slot_index]
        .set(jnp.arange(tokens_here * top_count, dtype=jnp.int32) // top_count)
    )
    padded = jnp.concatenate([normed, jnp.zeros((1, normed.shape[1]), jnp.bfloat16)], axis=0)
    outgoing = padded[owner_row].reshape(experts, capacity, normed.shape[1])
    expert_input = lax.all_gather(
        lax.all_to_all(outgoing, "sp", split_axis=0, concat_axis=0, tiled=True),
        "tp",
        axis=2,
        tiled=True,
    )
    sources = expert_input.shape[0]
    items = expert_input.shape[1]
    flat_rows = expert_input.reshape(sources * items, -1)
    pre_gate = jnp.dot(flat_rows, gate_weight[0], preferred_element_type=jnp.float32)
    pre_up = jnp.dot(flat_rows, up_weight[0], preferred_element_type=jnp.float32)
    capped = jnp.minimum(pre_gate, CLAMP_LIMIT)
    linear = jnp.clip(pre_up, -CLAMP_LIMIT, CLAMP_LIMIT)
    hidden = (capped * jax.nn.sigmoid(SWISH_ALPHA * capped) * (linear + 1.0)).astype(jnp.bfloat16)
    weight_slice = down_weight[0]
    expert_out = jnp.dot(
        lax.all_gather(hidden, "tp", axis=1, tiled=True),
        weight_slice,
        preferred_element_type=jnp.float32,
    )
    expert_out = expert_out.astype(jnp.bfloat16).reshape(sources, items, -1)
    returned_rows = lax.all_to_all(expert_out, "sp", split_axis=0, concat_axis=0, tiled=True)
    picked = returned_rows.reshape(experts * capacity, -1)[slot_index].astype(jnp.float32)
    picked = picked.reshape(tokens_here, top_count, -1)
    weights = jax.nn.softmax(route_logit, axis=-1)
    routed = jnp.sum(picked * weights[..., None], axis=1)
    return (mixer_float + routed).astype(jnp.bfloat16)


def solution(mesh):
    return jax.shard_map(
        local,
        mesh=mesh,
        in_specs=(
            P("sp", "tp"),
            P("sp", "tp", None),
            P("sp", "tp", None),
            P("sp", "tp", None),
            P("tp"),
            P(),
            P(None, "tp"),
            P(),
            P("sp", None, "tp"),
            P("sp", None, "tp"),
            P("sp", None, "tp"),
            P("sp", None),
            P("sp", None),
        ),
        out_specs=P("sp", "tp"),
        check_vma=False,
    )
```

profile of v0, /device:TPU:0, one launch (start us, length us, event | category | flops | bytes accessed | tf_op | source)
XLA Modules:
  0.0 296.3 jit_solution(3500172858010482587)
XLA Ops:
  6.5 1.8 copy.27
  8.4 1.6 copy.29
  10.1 0.8 copy.34
  10.9 0.1 eq.29
  11.1 0.1 eq.25
  11.2 0.2 fusion.56
  11.4 0.1 copy.37
  11.6 0.1 copy.38
  11.8 0.9 reduce-window.6
  12.6 0.2 slice_reduce_fusion
  13.0 0.1 mul.173
  13.2 0.8 dynamic_slice.28
  14.1 2.9 scatter_custom_fusion
  17.0 39.5 %all-gather.5.cloned.1.call-done = bf16[1536,4,128]{2,0,1:T(8,128)(2,1)} async-done(((bf16[192,4,128]{2,0,1:T(8,128)(2,1)}), bf16[1536,4,128]{2,0,1:T(8,128)(2,1)}) %all-gather.5.cloned.1.call-update) | async-done | bytes 1572880 | tf_op jit(solution)/shard_map/all_gather | solution.py:64
  56.5 2.6 copy.31
  59.1 42.2 %all-gather.7.cloned.1.call-done = bf16[1536,4,128]{2,0,1:T(8,128)(2,1)} async-done(((bf16[192,4,128]{2,0,1:T(8,128)(2,1)}), bf16[1536,4,128]{2,0,1:T(8,128)(2,1)}) %all-gather.7.cloned.1.call-update) | async-done | bytes 1572880 | tf_op jit(solution)/shard_map/all_gather | solution.py:65
  101.2 2.7 copy.32
  104.0 9.0 %while.23 = (s32[]{:T(128)}, f32[4,192]{1,0:T(4,128)S(1)}, f32[4,192]{1,0:T(4,128)S(1)}, f32[4,192,128]{2,1,0:T(8,128)S(1)}, f32[4,192]{1,0:T(4,128)S(1)}, /*ind...) while((s32[]{:T(128)}, f32[4,192]{1,0:T(4,128)S(1)}, ...), condition=%wide.region_7.8_spmd.clone, body=%wide.region_0.7_spmd.clone.sunk | while | flops 309574784 | bytes 20891532 | solution.py:88
  104.1 0.6 dynamic_slice.42
  105.4 5.0 %conditional.3 = ((f32[4,192]{1,0:T(4,128)S(1)}, f32[4,192]{1,0:T(4,128)S(1)}, f32[4,192,128]{2,1,0:T(8,128)S(1)}, f32[4,192]{1,0:T(4,128)S(1)}, f32[4,192]{1,0:T(4,128)S(1)}, /*index=5*/f32[4,192,128]{2,1,0:T(8,128)S(1)})) conditional(s32[]{:T(128)} %convert_element_type.82, (f32[4,192]{1,0:T(4,128)S(1)}, f32[4,192]{1,0:T(4,128)S(1)}, ...), branch_computations={%region_1.1_spmd, %region_2.6_spmd.clone} | conditional | flops 309572096 | bytes 20887848 | solution.py:83
  105.5 1.1 dynamic-slice_bitcast_fusion
  106.6 0.6 fusion.54
  107.2 0.6 fusion.55
  107.8 1.2 fusion.5
  109.0 0.2 copy-done.1
  109.2 0.6 convolution_add_fusion
  109.7 0.6 convolution_add_fusion.1
  110.4 0.6 dynamic_slice.42
  111.7 0.6 dynamic_slice.42
  113.1 0.5 multiply_reduce_fusion.2
  113.6 0.2 multiply_convert_fusion.2
  113.7 8.6 %all_gather.17 = bf16[16,192,128]{2,1,0:T(8,128)(2,1)S(1)} all-gather(bf16[4,192,128]{2,1,0:T(8,128)(2,1)S(1)} %multiply_convert_fusion.2), channel_id=1, replica_groups=mesh['sp'=8,'tp'=4] {'tp'}, dimensions={0}, use_global_device_ids=true | all-gather | bytes 983040 | tf_op jit(solution)/shard_map/all_gather | solution.py:103
  122.3 0.7 multiply_reduce_fusion.1
  123.0 6.2 %psum.7 = f32[192]{0:T(256)S(1)} all-reduce(f32[192]{0:T(256)S(1)} %get-tuple-element.467), channel_id=1, replica_groups=mesh['sp'=8,'tp'=4] {'tp'}, use_global_device_ids=true, to_apply=%region_10.11 | all-reduce | flops 192 | bytes 1536 | tf_op jit(solution)/shard_map/psum | solution.py:110
  129.3 2.7 gather_fusion
  132.0 32.5 %all_to_all.10 = bf16[8,96,512]{2,1,0:T(8,128)(2,1)} all-to-all(bf16[8,96,512]{2,1,0:T(8,128)(2,1)S(1)} %bitcast.62), channel_id=1, replica_groups=mesh['sp'=8,'tp'=4] {'sp'}, dimensions={0} | all-to-all | bytes 1572864 | tf_op jit(solution)/shard_map/all_to_all | solution.py:132
  164.5 0.2 all-gather.11.cloned.1.call-start
  164.7 26.5 %all-gather.9.cloned.1.call-done = bf16[8,96,2048]{2,1,0:T(8,128)(2,1)} async-done(((bf16[8,96,512]{2,1,0:T(8,128)(2,1)}), bf16[8,96,2048]{2,1,0:T(8,128)(2,1)}) %all-gather.9.cloned.1.call-update) | async-done | bytes 3145744 | tf_op jit(solution)/shard_map/all_gather | solution.py:131
  191.3 6.3 %fusion.32 = f32[768,1024]{1,0:T(8,128)S(1)} fusion(bf16[768,2048]{1,0:T(8,128)(2,1)} %bitcast.67, bf16[1,2048,1024]{2,1,0:T(8,128)(2,1)} %param.26), kind=kOutput, calls=%fused_computation.55 | convolution fusion | flops 3221225472 | bytes 10485760 | tf_op jit(solution)/shard_map/dot_general | solution.py:141
  197.6 5.3 %multiply_convert_fusion = bf16[768,1024]{1,0:T(8,128)(2,1)} fusion(f32[768,1024]{1,0:T(8,128)S(1)} %fusion.32, bf16[768,2048]{1,0:T(8,128)(2,1)S(1)} %bitcast.68, bf16[1,2048,1024]{2,1,0:T(8,128)(2,1)S(1)} %copy-done.8), kind=kOutput, calls=%fused_computation.59 | convolution fusion | flops 3229089792 | bytes 12058624 | tf_op jit(solution)/shard_map/dot_general | solution.py:140
  202.9 46.5 %all-gather.11.cloned.1.call-done = bf16[768,4096]{1,0:T(8,128)(2,1)} async-done(((bf16[768,1024]{1,0:T(8,128)(2,1)}), bf16[768,4096]{1,0:T(8,128)(2,1)}) %all-gather.11.cloned.1.call-update) | async-done | bytes 6291472 | tf_op jit(solution)/shard_map/all_gather | solution.py:147
  249.4 8.3 %fusion.38 = bf16[768,512]{1,0:T(8,128)(2,1)} fusion(bf16[768,4096]{1,0:T(8,128)(2,1)} %all-gather.11.cloned.1.call-done, bf16[1,4096,512]{2,1,0:T(8,128)(2,1)} %param.27), kind=kOutput, calls=%fused_computation.60 | convolution fusion | flops 3221618688 | bytes 11272192 | tf_op jit(solution)/shard_map/dot_general | solution.py:146
  257.7 5.6 %all-to-all-start.1 = ((bf16[8,96,512]{2,1,0:T(8,128)(2,1)}), bf16[8,96,512]{2,1,0:T(8,128)(2,1)S(1)}, u32[]{:S(2)}, u32[]{:S(2)}) async-start(bf16[8,96,512]{2,1,0:T(8,128)(2,1)} %bitcast.65), calls=%async_computation.1 | async-start | bytes 1572864 | tf_op jit(solution)/shard_map/all_to_all | solution.py:152
  263.6 20.4 %all-to-all-done.1 = bf16[8,96,512]{2,1,0:T(8,128)(2,1)S(1)} async-done(((bf16[8,96,512]{2,1,0:T(8,128)(2,1)}), bf16[8,96,512]{2,1,0:T(8,128)(2,1)S(1)}, u32[]{:S(2)}, u32[]{:S(2)}) %all-to-all-start.1) | async-done | bytes 786464 | tf_op jit(solution)/shard_map/all_to_all | solution.py:152
  283.9 2.6 gather_fusion.1
  286.5 1.5 reshape.153
  288.0 1.0 multiply_reduce_fusion
  289.0 0.7 add_convert_fusion
  (74 shorter events, 1.2 us)
Async XLA Ops:
  6.5 115.8 %copy-start = (bf16[2048,512]{1,0:T(8,128)(2,1)S(1)}, bf16[2048,512]{1,0:T(8,128)(2,1)}, u32[]{:S(2)}) copy-start(bf16[2048,512]{1,0:T(8,128)(2,1)} %param.23) | copy-start | bytes 6291460
  6.5 6.4 %copy-start.5 = (s32[192,2]{0,1:T(2,128)S(1)}, s32[192,2]{0,1:T(2,128)}, u32[]{:S(2)}) copy-start(s32[192,2]{0,1:T(2,128)} %param.28) | copy-start | bytes 4612
  6.5 4.7 %copy-start.2 = (bf16[192,4,128]{2,1,0:T(4,128)(2,1)S(1)}, bf16[192,4,128]{2,1,0:T(4,128)(2,1)}, u32[]{:S(2)}) copy-start(bf16[192,4,128]{2,1,0:T(4,128)(2,1)} %param.18) | copy-start | bytes 589828
  6.5 49.9 %all-gather.5.cloned.1.call-start = ((), (), s32[]{:S(2)}) async-start(), calls=%async_computation.2 | async-start | bytes 1769472 | tf_op jit(solution)/shard_map/all_gather | solution.py:64
  8.4 92.9 %all-gather.7.cloned.1.call-start = ((), (), s32[]{:S(2)}) async-start(), calls=%async_computation.3 | async-start | bytes 1769472 | tf_op jit(solution)/shard_map/all_gather | solution.py:65
  10.1 181.2 %all-gather.9.cloned.1.call-start = ((), (), s32[]{:S(2)}) async-start(), calls=%async_computation.4 | async-start | bytes 3932160 | tf_op jit(solution)/shard_map/all_gather | solution.py:131
  104.0 9.0 %copy-start.6 = (f32[4]{0:T(128)S(1)}, f32[4]{0:T(128)}, u32[]{:S(2)}) copy-start(f32[4]{0:T(128)} %param.21) | copy-start | bytes 52
  104.0 9.5 %copy-start.7 = (f32[128]{0:T(128)S(1)}, f32[128]{0:T(128)}, u32[]{:S(2)}) copy-start(f32[128]{0:T(128)} %param.22) | copy-start | bytes 1540
  107.8 1.4 copy-start.1
  113.0 9.3 %copy-start.3 = (bf16[192,512]{1,0:T(8,128)(2,1)S(1)}, bf16[192,512]{1,0:T(8,128)(2,1)}, u32[]{:S(2)}) copy-start(bf16[192,512]{1,0:T(8,128)(2,1)} %param.17) | copy-start | bytes 589828
  164.5 84.9 %all-gather.11.cloned.1.call-start = ((), (), s32[]{:S(2)}) async-start(), calls=%async_computation.5 | async-start | bytes 7864320 | tf_op jit(solution)/shard_map/all_gather | solution.py:147
  191.2 6.3 %copy-start.8 = (bf16[1,2048,1024]{2,1,0:T(8,128)(2,1)S(1)}, bf16[1,2048,1024]{2,1,0:T(8,128)(2,1)}, u32[]{:S(2)}) copy-start(bf16[1,2048,1024]{2,1,0:T(8,128)(2,1)} %param.25) | copy-start | bytes 12582916
  191.3 6.3 %copy-start.9 = (bf16[8,96,2048]{2,1,0:T(8,128)(2,1)S(1)}, bf16[8,96,2048]{2,1,0:T(8,128)(2,1)}, u32[]{:S(2)}) copy-start(bf16[8,96,2048]{2,1,0:T(8,128)(2,1)} %all-gather.9.cloned.1.call-done) | copy-start | bytes 9437188
  257.7 5.7 %copy-start.4 = (f32[192,2]{0,1:T(2,128)S(1)}, f32[192,2]{0,1:T(2,128)}, u32[]{:S(2)}) copy-start(f32[192,2]{0,1:T(2,128)} %param.29) | copy-start | bytes 4612
  257.7 26.2 %all-to-all-start.1 = ((bf16[8,96,512]{2,1,0:T(8,128)(2,1)}), bf16[8,96,512]{2,1,0:T(8,128)(2,1)S(1)}, u32[]{:S(2)}, u32[]{:S(2)}) async-start(bf16[8,96,512]{2,1,0:T(8,128)(2,1)} %bitcast.65), calls=%async_computation.1 | async-start | bytes 1572864 | tf_op jit(solution)/shard_map/all_to_all | solution.py:152
Sparse Core Ops, SparseCore 0:
  9.5 46.9 all-gather.4
  58.7 42.5 all-gather.6
  164.6 26.5 all-gather.8
  203.0 46.3 all-gather.10
where the time goes:
time: 297 us; the launch traced here: 296 us
  waiting for transfers between devices  175 us (59%)
  blocking collectives  47.2 us (16%)
  local copies, waits for them, and re-layouts  24.5 us (8%)
  matrix products  22.8 us (8%)
  between operations  13.4 us (5%)
  starting transfers between devices  5.96 us (2%)
  other arithmetic  5.09 us (2%)
    all_gather x1, waiting for transfers between devices, local(): lax.all_gather(hidden, 'tp', axis=1, tiled=True)  46.5 us
    all_gather x1, waiting for transfers between devices, local(): value_piece = lax.all_gather(value_rows, 'sp', axis=0, tiled=True)  42.2 us
    all_gather x1, waiting for transfers between devices, local(): key_piece = lax.all_gather(key_rows, 'sp', axis=0, tiled=True)  39.5 us
    all_to_all x1, blocking collectives, local(): lax.all_to_all(outgoing, 'sp', split_axis=0, concat_axis=0, tiled=True)  32.5 us
    all_gather x1, waiting for transfers between devices, local(): lax.all_gather(lax.all_to_all(outgoing, 'sp', split_axis=0, concat_axis=0...  26.5 us
    all_to_all x1, waiting for transfers between devices, local(): lax.all_to_all(expert_out, 'sp', split_axis=0, concat_axis=0, tiled=True)  20.4 us
    unnamed x25, local copies, waits for them, and re-layouts  9.82 us
    all_gather x1, blocking collectives, local(): lax.all_gather(attended, 'tp', axis=0, tiled=True)  8.58 us
  transfers between devices with their start and end apart: 5, of which 5 were waited for; matrix products, arithmetic and copies ran while one was open for 4% of the time, Pallas kernels for 0%

commit v1 on v0

--- a/solution.py
+++ b/solution.py
@@ -1,3 +1,4 @@
+import functools
 import math
 import jax
 import jax.numpy as jnp
@@ -12,6 +13,21 @@
 SWISH_ALPHA = 1.702
 HEAD_KEEP = 0.8
 NEG_FILL = -1e30
+
+
+def values_register(local_x, axis_key):
+    how_many = lax.axis_size(axis_key)
+    arr_now = [None] * how_many
+    arr_now[how_many - 1] = local_x
+    buffer = [(it, (it + 1) % how_many) for it in range(how_many)]
+    for kk in range(how_many - 2, -1, -1):
+        arr_now[kk] = lax.ppermute(arr_now[kk + 1], axis_key, buffer)
+    arr_out = jnp.concatenate(arr_now, axis=0)
+    answer = (lax.axis_index(axis_key) + 1) * local_x.shape[0]
+    return jnp.roll(arr_out, shift=answer, axis=0)
+
+
+guide_terms = functools.partial(values_register, axis_key="sp")
 
 
 def update_map(running, query_half, key_half, value_block, visible):
@@ -61,7 +77,7 @@
         jnp.zeros((heads_here, tokens_here, value_width), jnp.float32),
     )
     folded = (empty_map, empty_map)
-    key_piece = lax.all_gather(key_rows, "sp", axis=0, tiled=True)
+    key_piece = guide_terms(key_rows)
     value_piece = lax.all_gather(value_rows, "sp", axis=0, tiled=True)
     key_count = key_piece.shape[0]
     key_width = math.gcd(key_count, 1024)

time: 297 us -> 278 us (0.936)
  waiting for transfers between devices: 175 us -> 146 us
  local copies, waits for them, and re-layouts: 24.5 us -> 33.6 us
    ppermute x0 -> x7, waiting for transfers between devices: none -> 52 us  [values_register(): arr_now[kk] = lax.ppermute(arr_now[kk + 1], axis_key, buffer)]
    all_gather x1, waiting for transfers between devices: 42.2 us -> 0.01 us  [local(): value_piece = lax.all_gather(value_rows, 'sp', axis=0, tiled=True)]
    all_gather x1 -> x0, waiting for transfers between devices: 39.5 us -> none  [local(): key_piece = lax.all_gather(key_rows, 'sp', axis=0, tiled=True)]
    unnamed x25 -> x40, local copies, waits for them, and re-layouts: 9.82 us -> 15.8 us
    ppermute x0 -> x7, starting transfers between devices: none -> 3.04 us  [values_register(): arr_now[kk] = lax.ppermute(arr_now[kk + 1], axis_key, buffer)]
  transfers between devices with their start and end apart: 5 -> 11, of which waited for: 5 -> 10; matrix products, arithmetic and copies ran while one was open for 4% -> 8% of each run, Pallas kernels for 0% -> 0%
where the time goes in v1:
time: 278 us
  waiting for transfers between devices  146 us (53%)
  blocking collectives  44.9 us (16%)
  local copies, waits for them, and re-layouts  33.6 us (12%)
  matrix products  22.8 us (8%)
  between operations  13.5 us (5%)
  starting transfers between devices  8.82 us (3%)
  other arithmetic  5.77 us (2%)
    ppermute x7, waiting for transfers between devices, values_register(): arr_now[kk] = lax.ppermute(arr_now[kk + 1], axis_key, buffer)  52 us
    all_gather x1, waiting for transfers between devices, local(): lax.all_gather(hidden, 'tp', axis=1, tiled=True)  46.5 us
    all_to_all x1, blocking collectives, local(): lax.all_to_all(outgoing, 'sp', split_axis=0, concat_axis=0, tiled=True)  30.2 us
    all_gather x1, waiting for transfers between devices, local(): lax.all_gather(lax.all_to_all(outgoing, 'sp', split_axis=0, concat_axis=0...  27 us
    all_to_all x1, waiting for transfers between devices, local(): lax.all_to_all(expert_out, 'sp', split_axis=0, concat_axis=0, tiled=True)  20.4 us
    unnamed x40, local copies, waits for them, and re-layouts  15.8 us
    all_gather x1, blocking collectives, local(): lax.all_gather(attended, 'tp', axis=0, tiled=True)  8.61 us
    dot_general x1, matrix products, local(): jnp.dot(lax.all_gather(hidden, 'tp', axis=1, tiled=True), weight_slice, p...  8.3 us
  transfers between devices with their start and end apart: 11, of which 10 were waited for; matrix products, arithmetic and copies ran while one was open for 8% of the time, Pallas kernels for 0%

profile of v1, /device:TPU:0, one launch (start us, length us, event | category | flops | bytes accessed | tf_op | source)
XLA Modules:
  0.0 277.5 jit_solution(3017264992284718783)
XLA Ops:
  6.5 1.1 copy.29
  7.7 3.0 %collective-permute-start = (bf16[192,4,128]{2,0,1:T(8,128)(2,1)S(1)}, bf16[192,4,128]{2,0,1:T(8,128)(2,1)S(1)}, u32[]{:S(2)}, u32[]{:S(2)}) collective-permute-start(bf16[192,4,128]{2,0,1:T(8,128)(2,1)S(1)} %copy.29), channel_id=1, source_target_pairs={{0,4},{4,8},{8,12},{12,16},{16,20},{20,24},{24,28},{28,0},{1,5},{5... | collective-permute-start | bytes 589832 | tf_op jit(solution)/shard_map/ppermute | solution.py:24
  10.7 1.6 copy.33
  12.4 0.8 copy.38
  13.5 0.9 reduce-window.6
  14.4 4.3 %collective-permute-done = bf16[192,4,128]{2,0,1:T(8,128)(2,1)S(1)} collective-permute-done((bf16[192,4,128]{2,0,1:T(8,128)(2,1)S(1)}, bf16[192,4,128]{2,0,1:T(8,128)(2,1)S(1)}, u32[]{:S(2)}, u32[]{:S(2)}) %collective-permute-start) | collective-permute-done | bytes 196640 | tf_op jit(solution)/shard_map/ppermute | solution.py:24
  18.6 0.7 broadcast_multiply_fusion
  19.3 10.1 %collective-permute-done.1 = bf16[192,4,128]{2,0,1:T(8,128)(2,1)S(1)} collective-permute-done((bf16[192,4,128]{2,0,1:T(8,128)(2,1)S(1)}, bf16[192,4,128]{2,0,1:T(8,128)(2,1)S(1)}, u32[]{:S(2)}, u32[]{:S(2)}) %collective-permute-start.1) | collective-permute-done | bytes 196640 | tf_op jit(solution)/shard_map/ppermute | solution.py:24
  30.0 7.9 %collective-permute-done.2 = bf16[192,4,128]{2,0,1:T(8,128)(2,1)S(1)} collective-permute-done((bf16[192,4,128]{2,0,1:T(8,128)(2,1)S(1)}, bf16[192,4,128]{2,0,1:T(8,128)(2,1)S(1)}, u32[]{:S(2)}, u32[]{:S(2)}) %collective-permute-start.2) | collective-permute-done | bytes 196640 | tf_op jit(solution)/shard_map/ppermute | solution.py:24
  37.9 1.9 fusion.56
  39.9 6.7 %collective-permute-done.3 = bf16[192,4,128]{2,0,1:T(8,128)(2,1)S(1)} collective-permute-done((bf16[192,4,128]{2,0,1:T(8,128)(2,1)S(1)}, bf16[192,4,128]{2,0,1:T(8,128)(2,1)S(1)}, u32[]{:S(2)}, u32[]{:S(2)}) %collective-permute-start.3) | collective-permute-done | bytes 196640 | tf_op jit(solution)/shard_map/ppermute | solution.py:24
  46.5 12.4 %collective-permute-done.4 = bf16[192,4,128]{2,0,1:T(8,128)(2,1)S(1)} collective-permute-done((bf16[192,4,128]{2,0,1:T(8,128)(2,1)S(1)}, bf16[192,4,128]{2,0,1:T(8,128)(2,1)S(1)}, u32[]{:S(2)}, u32[]{:S(2)}) %collective-permute-start.4) | collective-permute-done | bytes 196640 | tf_op jit(solution)/shard_map/ppermute | solution.py:24
  59.0 2.9 %scatter_custom_fusion = s32[768]{0:T(1024)S(1)} fusion(s32[384]{0:T(512)S(1)} %fusion.51, s32[384]{0:T(512)S(1)} %add_select_fusion.1, s32[]{:T(128)} %constant.159.clone.1), kind=kCustom, calls=%fused_computation.106 | custom fusion | bytes 3076 | tf_op jit(solution)/shard_map/scatter | solution.py:143
  61.9 5.5 %collective-permute-done.5 = bf16[192,4,128]{2,0,1:T(8,128)(2,1)} collective-permute-done((bf16[192,4,128]{2,0,1:T(8,128)(2,1)S(1)}, bf16[192,4,128]{2,0,1:T(8,128)(2,1)}, u32[]{:S(2)}, u32[]{:S(2)}) %collective-permute-start.5) | collective-permute-done | bytes 196640 | tf_op jit(solution)/shard_map/ppermute | solution.py:24
  67.5 1.1 copy.41
  68.5 1.7 copy.42
  70.3 0.8 dynamic_slice.33
  71.0 5.1 %collective-permute-done.6 = bf16[192,4,128]{2,0,1:T(8,128)(2,1)} collective-permute-done((bf16[192,4,128]{2,0,1:T(8,128)(2,1)}, bf16[192,4,128]{2,0,1:T(8,128)(2,1)}, u32[]{:S(2)}, u32[]{:S(2)}) %collective-permute-start.6) | collective-permute-done | bytes 196640 | tf_op jit(solution)/shard_map/ppermute | solution.py:24
  76.1 0.9 constant_dynamic-update-slice_fusion.15
  77.1 1.0 constant_dynamic-update-slice_fusion.14
  78.3 1.0 constant_dynamic-update-slice_fusion.7
  79.3 1.0 constant_dynamic-update-slice_fusion.6
  80.4 1.6 constant_dynamic-slice_fusion
  82.0 2.6 copy.35
  84.6 2.6 copy.36
  87.4 8.8 %while.23 = (s32[]{:T(128)}, f32[4,192]{1,0:T(4,128)S(1)}, f32[4,192]{1,0:T(4,128)S(1)}, f32[4,192,128]{2,1,0:T(8,128)S(1)}, f32[4,192]{1,0:T(4,128)S(1)}, /*ind...) while((s32[]{:T(128)}, f32[4,192]{1,0:T(4,128)S(1)}, ...), condition=%wide.region_7.8_spmd.clone, body=%wide.region_0.7_spmd.clone.sunk | while | flops 309574784 | bytes 20891532 | solution.py:104
  87.5 0.6 dynamic_slice.48
  88.7 4.8 %conditional.3 = ((f32[4,192]{1,0:T(4,128)S(1)}, f32[4,192]{1,0:T(4,128)S(1)}, f32[4,192,128]{2,1,0:T(8,128)S(1)}, f32[4,192]{1,0:T(4,128)S(1)}, f32[4,192]{1,0:T(4,128)S(1)}, /*index=5*/f32[4,192,128]{2,1,0:T(8,128)S(1)})) conditional(s32[]{:T(128)} %convert_element_type.82, (f32[4,192]{1,0:T(4,128)S(1)}, f32[4,192]{1,0:T(4,128)S(1)}, ...), branch_computations={%region_1.1_spmd, %region_2.6_spmd.clone} | conditional | flops 309572096 | bytes 20887848 | solution.py:99
  88.9 1.1 dynamic-slice_bitcast_fusion
  91.2 1.2 fusion.5
  93.6 0.6 dynamic_slice.48
  95.0 0.6 dynamic_slice.48
  97.0 8.6 %all_gather.13 = bf16[16,192,128]{2,1,0:T(8,128)(2,1)S(1)} all-gather(bf16[4,192,128]{2,1,0:T(8,128)(2,1)S(1)} %multiply_convert_fusion.2), channel_id=1, replica_groups=mesh['sp'=8,'tp'=4] {'tp'}, dimensions={0}, use_global_device_ids=true | all-gather | bytes 983040 | tf_op jit(solution)/shard_map/all_gather | solution.py:119
  105.6 0.7 multiply_reduce_fusion.1
  106.3 6.1 %psum.7 = f32[192]{0:T(256)S(1)} all-reduce(f32[192]{0:T(256)S(1)} %get-tuple-element.467), channel_id=1, replica_groups=mesh['sp'=8,'tp'=4] {'tp'}, use_global_device_ids=true, to_apply=%region_10.11 | all-reduce | flops 192 | bytes 1536 | tf_op jit(solution)/shard_map/psum | solution.py:126
  112.5 2.7 gather_fusion
  115.2 30.2 %all_to_all.10 = bf16[8,96,512]{2,1,0:T(8,128)(2,1)} all-to-all(bf16[8,96,512]{2,1,0:T(8,128)(2,1)S(1)} %bitcast.63), channel_id=1, replica_groups=mesh['sp'=8,'tp'=4] {'sp'}, dimensions={0} | all-to-all | bytes 1572864 | tf_op jit(solution)/shard_map/all_to_all | solution.py:148
  145.6 27.0 %all-gather.6.cloned.1.call-done = bf16[8,96,2048]{2,1,0:T(8,128)(2,1)} async-done(((bf16[8,96,512]{2,1,0:T(8,128)(2,1)}), bf16[8,96,2048]{2,1,0:T(8,128)(2,1)}) %all-gather.6.cloned.1.call-update) | async-done | bytes 3145744 | tf_op jit(solution)/shard_map/all_gather | solution.py:147
  172.6 6.3 %fusion.32 = f32[768,1024]{1,0:T(8,128)S(1)} fusion(bf16[768,2048]{1,0:T(8,128)(2,1)} %bitcast.67, bf16[1,2048,1024]{2,1,0:T(8,128)(2,1)} %param.26), kind=kOutput, calls=%fused_computation.55 | convolution fusion | flops 3221225472 | bytes 10485760 | tf_op jit(solution)/shard_map/dot_general | solution.py:157
  179.0 5.3 %multiply_convert_fusion = bf16[768,1024]{1,0:T(8,128)(2,1)} fusion(f32[768,1024]{1,0:T(8,128)S(1)} %fusion.32, bf16[768,2048]{1,0:T(8,128)(2,1)S(1)} %bitcast.68, bf16[1,2048,1024]{2,1,0:T(8,128)(2,1)S(1)} %copy-done.8), kind=kOutput, calls=%fused_computation.59 | convolution fusion | flops 3229089792 | bytes 12058624 | tf_op jit(solution)/shard_map/dot_general | solution.py:156
  184.3 46.5 %all-gather.8.cloned.1.call-done = bf16[768,4096]{1,0:T(8,128)(2,1)} async-done(((bf16[768,1024]{1,0:T(8,128)(2,1)}), bf16[768,4096]{1,0:T(8,128)(2,1)}) %all-gather.8.cloned.1.call-update) | async-done | bytes 6291472 | tf_op jit(solution)/shard_map/all_gather | solution.py:163
  230.8 8.3 %fusion.38 = bf16[768,512]{1,0:T(8,128)(2,1)} fusion(bf16[768,4096]{1,0:T(8,128)(2,1)} %all-gather.8.cloned.1.call-done, bf16[1,4096,512]{2,1,0:T(8,128)(2,1)} %param.27), kind=kOutput, calls=%fused_computation.60 | convolution fusion | flops 3221618688 | bytes 11272192 | tf_op jit(solution)/shard_map/dot_general | solution.py:162
  239.1 5.5 %all-to-all-start.1 = ((bf16[8,96,512]{2,1,0:T(8,128)(2,1)}), bf16[8,96,512]{2,1,0:T(8,128)(2,1)S(1)}, u32[]{:S(2)}, u32[]{:S(2)}) async-start(bf16[8,96,512]{2,1,0:T(8,128)(2,1)} %bitcast.65), calls=%async_computation.1 | async-start | bytes 1572864 | tf_op jit(solution)/shard_map/all_to_all | solution.py:168
  244.8 20.4 %all-to-all-done.1 = bf16[8,96,512]{2,1,0:T(8,128)(2,1)S(1)} async-done(((bf16[8,96,512]{2,1,0:T(8,128)(2,1)}), bf16[8,96,512]{2,1,0:T(8,128)(2,1)S(1)}, u32[]{:S(2)}, u32[]{:S(2)}) %all-to-all-start.1) | async-done | bytes 786464 | tf_op jit(solution)/shard_map/all_to_all | solution.py:168
  265.2 2.6 gather_fusion.1
  267.8 1.5 reshape.153
  269.3 1.0 multiply_reduce_fusion
  270.3 0.7 add_convert_fusion
  (102 shorter events, 5.3 us)
Async XLA Ops:
  6.5 99.0 %copy-start = (bf16[2048,512]{1,0:T(8,128)(2,1)S(1)}, bf16[2048,512]{1,0:T(8,128)(2,1)}, u32[]{:S(2)}) copy-start(bf16[2048,512]{1,0:T(8,128)(2,1)} %param.23) | copy-start | bytes 6291460
  6.5 71.7 %copy-start.2 = (bf16[192,4,128]{2,1,0:T(4,128)(2,1)S(1)}, bf16[192,4,128]{2,1,0:T(4,128)(2,1)}, u32[]{:S(2)}) copy-start(bf16[192,4,128]{2,1,0:T(4,128)(2,1)} %param.19) | copy-start | bytes 589828
  6.5 78.1 %all-gather.4.cloned.1.call-start = ((), (), s32[]{:S(2)}) async-start(), calls=%async_computation.2 | async-start | bytes 1769472 | tf_op jit(solution)/shard_map/all_gather | solution.py:81
  7.7 11.0 %collective-permute-start = (bf16[192,4,128]{2,0,1:T(8,128)(2,1)S(1)}, bf16[192,4,128]{2,0,1:T(8,128)(2,1)S(1)}, u32[]{:S(2)}, u32[]{:S(2)}) collective-permute-start(bf16[192,4,128]{2,0,1:T(8,128)(2,1)S(1)} %copy.29), channel_id=1, source_target_pairs={{0,4},{4,8},{8,12},{12,16},{16,20},{20,24},{24,28},{28,0},{1,5},{5... | collective-permute-start | bytes 589832 | tf_op jit(solution)/shard_map/ppermute | solution.py:24
  12.3 160.3 %all-gather.6.cloned.1.call-start = ((), (), s32[]{:S(2)}) async-start(), calls=%async_computation.3 | async-start | bytes 3932160 | tf_op jit(solution)/shard_map/all_gather | solution.py:147
  18.6 10.8 %collective-permute-start.1 = (bf16[192,4,128]{2,0,1:T(8,128)(2,1)S(1)}, bf16[192,4,128]{2,0,1:T(8,128)(2,1)S(1)}, u32[]{:S(2)}, u32[]{:S(2)}) collective-permute-start(bf16[192,4,128]{2,0,1:T(8,128)(2,1)S(1)} %collective-permute-done), channel_id=1, source_target_pairs={{0,4},{4,8},{8,12},{12,16},{16,20},{20,24},{24,28},{28,0},{1,5},{5... | collective-permute-start | bytes 589832 | tf_op jit(solution)/shard_map/ppermute | solution.py:24
  29.4 8.5 %collective-permute-start.2 = (bf16[192,4,128]{2,0,1:T(8,128)(2,1)S(1)}, bf16[192,4,128]{2,0,1:T(8,128)(2,1)S(1)}, u32[]{:S(2)}, u32[]{:S(2)}) collective-permute-start(bf16[192,4,128]{2,0,1:T(8,128)(2,1)S(1)} %collective-permute-done.1), channel_id=1, source_target_pairs={{0,4},{4,8},{8,12},{12,16},{16,20},{20,24},{24,28},{28,0},{1,5},{5... | collective-permute-start | bytes 589832 | tf_op jit(solution)/shard_map/ppermute | solution.py:24
  37.9 8.6 %collective-permute-start.3 = (bf16[192,4,128]{2,0,1:T(8,128)(2,1)S(1)}, bf16[192,4,128]{2,0,1:T(8,128)(2,1)S(1)}, u32[]{:S(2)}, u32[]{:S(2)}) collective-permute-start(bf16[192,4,128]{2,0,1:T(8,128)(2,1)S(1)} %collective-permute-done.2), channel_id=1, source_target_pairs={{0,4},{4,8},{8,12},{12,16},{16,20},{20,24},{24,28},{28,0},{1,5},{5... | collective-permute-start | bytes 589832 | tf_op jit(solution)/shard_map/ppermute | solution.py:24
  46.5 12.4 %collective-permute-start.4 = (bf16[192,4,128]{2,0,1:T(8,128)(2,1)S(1)}, bf16[192,4,128]{2,0,1:T(8,128)(2,1)S(1)}, u32[]{:S(2)}, u32[]{:S(2)}) collective-permute-start(bf16[192,4,128]{2,0,1:T(8,128)(2,1)S(1)} %collective-permute-done.3), channel_id=1, source_target_pairs={{0,4},{4,8},{8,12},{12,16},{16,20},{20,24},{24,28},{28,0},{1,5},{5... | collective-permute-start | bytes 589832 | tf_op jit(solution)/shard_map/ppermute | solution.py:24
  59.0 8.5 %collective-permute-start.5 = (bf16[192,4,128]{2,0,1:T(8,128)(2,1)S(1)}, bf16[192,4,128]{2,0,1:T(8,128)(2,1)}, u32[]{:S(2)}, u32[]{:S(2)}) collective-permute-start(bf16[192,4,128]{2,0,1:T(8,128)(2,1)S(1)} %collective-permute-done.4), channel_id=1, source_target_pairs={{0,4},{4,8},{8,12},{12,16},{16,20},{20,24},{24,28},{28,0},{1,5},{5... | collective-permute-start | bytes 589832 | tf_op jit(solution)/shard_map/ppermute | solution.py:24
  67.5 8.7 %collective-permute-start.6 = (bf16[192,4,128]{2,0,1:T(8,128)(2,1)}, bf16[192,4,128]{2,0,1:T(8,128)(2,1)}, u32[]{:S(2)}, u32[]{:S(2)}) collective-permute-start(bf16[192,4,128]{2,0,1:T(8,128)(2,1)} %collective-permute-done.5), channel_id=1, source_target_pairs={{0,4},{4,8},{8,12},{12,16},{16,20},{20,24},{24,28},{28,0},{1,5},{5... | collective-permute-start | bytes 589832 | tf_op jit(solution)/shard_map/ppermute | solution.py:24
  82.0 5.4 %copy-start.4 = (bf16[192,4,64]{0,2,1:T(8,128)(2,1)S(1)}, bf16[192,4,64]{0,2,1:T(8,128)(2,1)}, u32[]{:S(2)}) copy-start(bf16[192,4,64]{0,2,1:T(8,128)(2,1)} %copy.42) | copy-start | bytes 294916
  87.4 8.9 %copy-start.6 = (f32[4]{0:T(128)S(1)}, f32[4]{0:T(128)}, u32[]{:S(2)}) copy-start(f32[4]{0:T(128)} %param.21) | copy-start | bytes 52
  87.4 9.4 %copy-start.7 = (f32[128]{0:T(128)S(1)}, f32[128]{0:T(128)}, u32[]{:S(2)}) copy-start(f32[128]{0:T(128)} %param.22) | copy-start | bytes 1540
  87.4 18.2 %copy-start.3 = (bf16[192,512]{1,0:T(8,128)(2,1)S(1)}, bf16[192,512]{1,0:T(8,128)(2,1)}, u32[]{:S(2)}) copy-start(bf16[192,512]{1,0:T(8,128)(2,1)} %param.17) | copy-start | bytes 589828
  90.6 1.8 copy-start.1
  145.4 85.4 %all-gather.8.cloned.1.call-start = ((), (), s32[]{:S(2)}) async-start(), calls=%async_computation.4 | async-start | bytes 7864320 | tf_op jit(solution)/shard_map/all_gather | solution.py:163
  172.6 6.3 %copy-start.8 = (bf16[1,2048,1024]{2,1,0:T(8,128)(2,1)S(1)}, bf16[1,2048,1024]{2,1,0:T(8,128)(2,1)}, u32[]{:S(2)}) copy-start(bf16[1,2048,1024]{2,1,0:T(8,128)(2,1)} %param.25) | copy-start | bytes 12582916
  172.6 6.3 %copy-start.9 = (bf16[8,96,2048]{2,1,0:T(8,128)(2,1)S(1)}, bf16[8,96,2048]{2,1,0:T(8,128)(2,1)}, u32[]{:S(2)}) copy-start(bf16[8,96,2048]{2,1,0:T(8,128)(2,1)} %all-gather.6.cloned.1.call-done) | copy-start | bytes 9437188
  184.3 60.3 %copy-start.5 = (f32[192,2]{0,1:T(2,128)S(1)}, f32[192,2]{0,1:T(2,128)}, u32[]{:S(2)}) copy-start(f32[192,2]{0,1:T(2,128)} %param.29) | copy-start | bytes 4612
  239.1 26.1 %all-to-all-start.1 = ((bf16[8,96,512]{2,1,0:T(8,128)(2,1)}), bf16[8,96,512]{2,1,0:T(8,128)(2,1)S(1)}, u32[]{:S(2)}, u32[]{:S(2)}) async-start(bf16[8,96,512]{2,1,0:T(8,128)(2,1)} %bitcast.65), calls=%async_computation.1 | async-start | bytes 1572864 | tf_op jit(solution)/shard_map/all_to_all | solution.py:168
Sparse Core Ops, SparseCore 0:
  12.5 51.0 all-gather.3
  145.5 27.0 all-gather.5
  184.4 46.3 all-gather.7
